TPU v7x, 32 devices: a whole 2x2x4 slice. The times are simulated.
32 devices in a mesh: grp: 2 (over y), kv: 4 (over z), tp: 4 (over x, core).
Axes of the slice: x: 2, y: 2, z: 4, core: 2. Of those that a mesh axis runs over, the one named last changes fastest.
Arguments:
- tokens: bfloat16 [32, 2048], P('grp', ('kv', 'tp')), parts along dimension 0, may hold values from -13 to 13, as said below
- state: float32 [32, 16, 128, 128], P(('grp', 'kv'), 'tp'), parts along dimension 0, may hold values from -0.6 to 0.6
- norm_gain: bfloat16 [2048], P('kv'), may hold values from 0.099609375 to 1.8984375
- w_query: bfloat16 [2048, 2048], P('kv', 'tp'), may hold values from -0.125 to 0.125
- w_key: bfloat16 [2048, 2048], P('kv', 'tp'), may hold values from -0.125 to 0.125
- w_value: bfloat16 [2048, 2048], P('kv', 'tp'), may hold values from -0.125 to 0.125
- w_beta: bfloat16 [2048, 16], replicated, may hold values from -0.125 to 0.125
- w_decay: bfloat16 [2048, 16], replicated, may hold values from -0.125 to 0.125
- a_log: float32 [16], P('tp'), may hold values from -3 to 1
- dt_bias: float32 [16], P('tp'), may hold values from -2 to 1
- head_gain: float32 [128], replicated, may hold values from 0.1 to 1.9
- w_out: bfloat16 [2048, 2048], P('tp', 'kv'), may hold values from -0.125 to 0.125
- mixer_gain: bfloat16 [2048], P('kv'), may hold values from 0.099609375 to 1.8984375
- w_up: bfloat16 [2048, 8192], P('kv', 'tp'), may hold values from -0.125 to 0.125
- w_down: bfloat16 [8192, 2048], P('tp', 'kv'), may hold values from -0.0625 to 0.0625
Outputs:
- mixed: bfloat16 [32, 2048], P('grp', ('kv', 'tp')), parts along dimension 0
- new_state: float32 [32, 16, 128, 128], P(('grp', 'kv'), 'tp'), parts along dimension 0
There are 2 independent parts, one for each index of `grp`. A program takes and returns all parts, laid end to end along the dimension named above; an argument that names none is the same for every part. Nothing has to cross between parts.
Inputs may be any that keep to these rules, and one draw needn't show every extreme that they name: `tokens`: activations of order one.
All inputs are finite; a program needn't handle non-finite values.
Results may differ from a plain program's by a relative error of at most 0.019.
Values may be sent and summed in bfloat16 or wider, within the bound.
A program may use at most 64 MiB of HBM per device.

v0:
```python
import jax
import jax.numpy as jnp
from jax import lax
from jax.sharding import PartitionSpec as P

D = 2048


epsilon = 1e-06


def dotted(left, right):
    return jnp.dot(left, right, preferred_element_type=jnp.float32)


def delta_update(
    query_pre, key_pre, value_pre, beta_pre, decay_pre, state, a_log, dt_bias, head_gain
):
    query = query_pre * lax.rsqrt(jnp.sum(query_pre * query_pre, axis=-1, keepdims=True) + epsilon)
    keyed = key_pre * lax.rsqrt(jnp.sum(key_pre * key_pre, axis=-1, keepdims=True) + epsilon)
    beta = jax.nn.sigmoid(beta_pre)
    decay = jnp.exp(-jnp.exp(a_log) * jax.nn.softplus(decay_pre + dt_bias))
    key_read = jnp.einsum("bhk,bhkv->bhv", keyed, state)
    query_read = jnp.einsum("bhk,bhkv->bhv", query, state)
    fresh = beta[..., None] * (value_pre - decay[..., None] * key_read)
    new_state = decay[..., None, None] * state + keyed[..., :, None] * fresh[..., None, :]
    intersection = jnp.sum(query * keyed, axis=-1)
    reading = decay[..., None] * query_read + intersection[..., None] * fresh
    normed = (
        reading
        * lax.rsqrt(jnp.mean(reading * reading, axis=-1, keepdims=True) + epsilon)
        * head_gain
    )
    return (normed.astype(jnp.bfloat16), new_state)


def local(
    tokens,
    state,
    norm_gain,
    w_query,
    w_key,
    w_value,
    w_beta,
    w_decay,
    a_log,
    dt_bias,
    head_gain,
    w_out,
    mixer_gain,
    w_up,
    w_down,
):
    seq_here = state.shape[0]
    heads_here = state.shape[1]
    head_size = state.shape[2]
    kv_index = lax.axis_index("kv")
    tp_index = lax.axis_index("tp")
    gathered = lax.all_gather(tokens, "tp", axis=1, tiled=True)
    block = gathered.shape[1]
    inputs = gathered.astype(jnp.float32)
    scaled = (inputs * norm_gain.astype(jnp.float32)).astype(jnp.bfloat16)
    partial_sq = jnp.sum(inputs * inputs, axis=1)
    beta_rows = lax.dynamic_slice(
        w_beta, (kv_index * block, tp_index * heads_here), (block, heads_here)
    )
    decay_rows = lax.dynamic_slice(
        w_decay, (kv_index * block, tp_index * heads_here), (block, heads_here)
    )
    query_part = dotted(scaled, w_query)
    key_part = dotted(scaled, w_key)
    value_part = dotted(scaled, w_value)
    beta_part = dotted(scaled, beta_rows)
    decay_part = dotted(scaled, decay_rows)
    square_all = lax.psum(partial_sq, "kv")
    square_sum = lax.dynamic_slice_in_dim(square_all, kv_index * seq_here, seq_here, 0)
    query_sum, key_sum, value_sum, beta_sum, decay_sum = (
        lax.psum_scatter(query_part, "kv", scatter_dimension=0, tiled=True),
        lax.psum_scatter(key_part, "kv", scatter_dimension=0, tiled=True),
        lax.psum_scatter(value_part, "kv", scatter_dimension=0, tiled=True),
        lax.psum_scatter(beta_part, "kv", scatter_dimension=0, tiled=True),
        lax.psum_scatter(decay_part, "kv", scatter_dimension=0, tiled=True),
    )
    first = lax.rsqrt(square_sum / D + epsilon)[:, None]
    query_pre = (first * query_sum).reshape(seq_here, heads_here, head_size)
    key_pre = (first * key_sum).reshape(seq_here, heads_here, head_size)
    value_pre = (first * value_sum).reshape(seq_here, heads_here, head_size)
    normed, new_state = delta_update(
        query_pre,
        key_pre,
        value_pre,
        first * beta_sum,
        first * decay_sum,
        state,
        a_log,
        dt_bias,
        head_gain,
    )
    normed = normed.reshape(seq_here, heads_here * head_size)
    head_part = dotted(lax.all_gather(normed, "kv", axis=0, tiled=True), w_out)
    attended = lax.psum_scatter(
        head_part.astype(jnp.bfloat16), "tp", scatter_dimension=1, tiled=True
    ).astype(jnp.float32)
    middle = (tokens.astype(jnp.float32) + attended).astype(jnp.bfloat16)
    middle_rows = lax.all_gather(middle, "tp", axis=1, tiled=True).astype(jnp.float32)
    square_two = lax.psum(jnp.sum(middle_rows * middle_rows, axis=1), "kv")
    second = lax.rsqrt(square_two / D + epsilon)[:, None]
    scaled_two = (middle_rows * mixer_gain.astype(jnp.float32)).astype(jnp.bfloat16)
    up_part = dotted(scaled_two, w_up)
    up_share = lax.psum_scatter(up_part, "kv", scatter_dimension=1, tiled=True)
    hidden_share = jnp.square(jax.nn.relu(second * up_share)).astype(jnp.bfloat16)
    down_part = dotted(lax.all_gather(hidden_share, "kv", axis=1, tiled=True), w_down)
    lowered = lax.psum_scatter(
        down_part.astype(jnp.bfloat16), "tp", scatter_dimension=1, tiled=True
    ).astype(jnp.float32)
    mixed = (middle.astype(jnp.float32) + lowered).astype(jnp.bfloat16)
    return (mixed, new_state)


def solution(mesh):
    return jax.shard_map(
        local,
        mesh=mesh,
        in_specs=(
            P("grp", ("kv", "tp")),
            P(("grp", "kv"), "tp", None, None),
            P("kv"),
            P("kv", "tp"),
            P("kv", "tp"),
            P("kv", "tp"),
            P(),
            P(),
            P("tp"),
            P("tp"),
            P(),
            P("tp", "kv"),
            P("kv"),
            P("kv", "tp"),
            P("tp", "kv"),
        ),
        out_specs=(P("grp", ("kv", "tp")), P(("grp", "kv"), "tp", None, None)),
        check_vma=False,
    )
```

profile of v0, /device:TPU:0, one launch (start us, length us, event | category | flops | bytes accessed | tf_op | source)
XLA Modules:
  0.0 168.6 jit_solution(6486688336982483888)
XLA Ops:
  7.3 0.8 convert_element_type.50
  8.1 6.5 %all_gather.12 = bf16[16,512]{1,0:T(8,128)(2,1)S(1)} all-gather(bf16[16,128]{1,0:T(8,128)(2,1)} %param.15), channel_id=1, replica_groups=mesh['grp'=2,'kv'=4,'tp'=4] {'tp'}, dimensions={1}, use_global_device_ids=true | all-gather | bytes 20480 | tf_op jit(solution)/shard_map/all_gather | solution.py:59
  14.6 0.6 fusion.3
  15.2 1.5 fusion.12
  16.7 1.5 fusion.18
  18.2 1.8 %fusion.16 = f32[16,512]{1,0:T(8,128)} fusion(bf16[512,512]{1,0:T(8,128)(2,1)} %param.18, bf16[16,512]{1,0:T(8,128)(2,1)S(1)} %all_gather.12, f32[512]{0:T(512)S(1)} %convert_element_type.50), kind=kOutput, calls=%fused_computation.31 | convolution fusion | flops 8413184 | bytes 575488 | tf_op jit(solution)/shard_map/dot_general | solution.py:13
  20.0 1.8 %fusion.14 = f32[16,512]{1,0:T(8,128)} fusion(bf16[512,512]{1,0:T(8,128)(2,1)} %param.19, bf16[16,512]{1,0:T(8,128)(2,1)S(1)} %all_gather.12, f32[512]{0:T(512)S(1)} %convert_element_type.50), kind=kOutput, calls=%fused_computation.30 | convolution fusion | flops 8413184 | bytes 575488 | tf_op jit(solution)/shard_map/dot_general | solution.py:13
  21.9 1.9 %fusion.10 = f32[16,512]{1,0:T(8,128)} fusion(bf16[512,512]{1,0:T(8,128)(2,1)} %param.20, bf16[16,512]{1,0:T(8,128)(2,1)S(1)} %all_gather.12, f32[512]{0:T(512)S(1)} %convert_element_type.50), kind=kOutput, calls=%fused_computation.28 | convolution fusion | flops 8413184 | bytes 575488 | tf_op jit(solution)/shard_map/dot_general | solution.py:13
  23.8 0.7 exponential_negate_fusion
  24.5 1.3 dynamic-slice
  26.4 34.2 %all-reduce.8.cloned.1.call-done = (f32[16,512]{1,0:T(8,128)}, f32[16]{0:T(128)}, f32[16,512]{1,0:T(8,128)}, f32[16,4]{1,0:T(8,128)}, f32[16,4]{1,0:T(8,128)}, /*index=5*/f32[16,512]{1,0:T(8,128)}) async-done(((f32[16,512]{1,0:T(8,128)}, f32[16]{0:T(128)}, f32[16,512]{1,0:T(8,128)}, f32[16,4]{1,0:T(8,128)}, f32[16,4]{1,0:T(8,128)}, /*index=5*/f32[16,512]{1,0:T(8,128)}), (f32[16,512]{1,0:T(8,128)}, ...) | async-done | bytes 98896
  60.6 0.7 add_rsqrt_fusion.4
  61.3 0.8 dynamic-slice_multiply_fusion.2
  62.7 0.8 fusion.24
  63.6 0.3 fusion.30
  64.1 13.3 %all-gather = bf16[4,4,512]{2,1,0:T(4,128)(2,1)S(1)} all-gather(bf16[1,4,512]{2,1,0:T(4,128)(2,1)S(1)} %reshape.57), channel_id=1, replica_groups=mesh['grp'=2,'kv'=4,'tp'=4] {'kv'}, dimensions={0}, use_global_device_ids=true | all-gather | bytes 20480 | tf_op jit(solution)/shard_map/all_gather | solution.py:100
  77.4 1.2 convolution_convert_fusion.1
  78.6 0.8 copy.21
  79.5 19.8 %reduce-scatter.10.cloned.1.call-done = bf16[128,16]{1,0:T(8,128)(2,1)} async-done(((bf16[512,16]{1,0:T(8,128)(2,1)}), bf16[128,16]{1,0:T(8,128)(2,1)}) %reduce-scatter.10.cloned.1.call-update) | async-done | bytes 4112
  99.3 0.8 copy.22
  100.1 5.2 %all_gather.14 = bf16[16,512]{1,0:T(8,128)(2,1)S(1)} all-gather(bf16[16,128]{1,0:T(8,128)(2,1)S(1)} %add_convert_fusion.1), channel_id=1, replica_groups=mesh['grp'=2,'kv'=4,'tp'=4] {'tp'}, dimensions={1}, use_global_device_ids=true | all-gather | bytes 20480 | tf_op jit(solution)/shard_map/all_gather | solution.py:105
  105.3 1.0 fusion.7
  106.5 11.7 %psum.15 = f32[16]{0:T(128)S(1)} all-reduce(f32[16]{0:T(128)S(1)} %fusion.5), channel_id=1, replica_groups=mesh['grp'=2,'kv'=4,'tp'=4] {'kv'}, use_global_device_ids=true, to_apply=%region_13.14 | all-reduce | flops 16 | bytes 128 | tf_op jit(solution)/shard_map/psum | solution.py:106
  118.3 7.7 %reduce-scatter.8.cloned.1.call-done = f32[16,512]{1,0:T(8,128)} async-done(((f32[16,2048]{1,0:T(8,128)}), f32[16,512]{1,0:T(8,128)}) %reduce-scatter.8.cloned.1.call-update) | async-done | bytes 32784 | tf_op jit(solution)/shard_map/reduce_scatter | solution.py:110
  126.0 0.8 multiply_convert_fusion
  126.8 13.1 %all_gather.15 = bf16[16,2048]{1,0:T(8,128)(2,1)S(1)} all-gather(bf16[16,512]{1,0:T(8,128)(2,1)S(1)} %multiply_convert_fusion), channel_id=1, replica_groups=mesh['grp'=2,'kv'=4,'tp'=4] {'kv'}, dimensions={1}, use_global_device_ids=true | all-gather | bytes 81920 | tf_op jit(solution)/shard_map/all_gather | solution.py:112
  139.9 2.0 %convolution_convert_fusion = bf16[16,512]{1,0:T(8,128)(2,1)S(1)} fusion(bf16[16,2048]{1,0:T(8,128)(2,1)S(1)} %all_gather.15, bf16[2048,512]{1,0:T(8,128)(2,1)} %param.29), kind=kOutput, calls=%fused_computation.1 | convolution fusion | flops 33562624 | bytes 2179072 | tf_op jit(solution)/shard_map/dot_general | solution.py:13
  141.9 0.8 copy.23
  142.7 1.3 multiply_add_fusion
  144.0 16.7 %reduce-scatter.12.cloned.1.call-done = bf16[128,16]{1,0:T(8,128)(2,1)} async-done(((bf16[512,16]{1,0:T(8,128)(2,1)}), bf16[128,16]{1,0:T(8,128)(2,1)}) %reduce-scatter.12.cloned.1.call-update) | async-done | bytes 4112
  160.7 0.8 copy.24
  161.5 0.6 add_convert_fusion
  (39 shorter events, 1.3 us)
Async XLA Ops:
  7.2 98.1 %copy-start = (bf16[512,2048]{1,0:T(8,128)(2,1)S(1)}, bf16[512,2048]{1,0:T(8,128)(2,1)}, u32[]{:S(2)}) copy-start(bf16[512,2048]{1,0:T(8,128)(2,1)} %param.28) | copy-start | bytes 6291460
  7.2 55.3 %copy-start.1 = (f32[4,4,128,128]{3,2,1,0:T(8,128)S(1)}, f32[4,4,128,128]{3,2,1,0:T(8,128)}, u32[]{:S(2)}) copy-start(f32[4,4,128,128]{3,2,1,0:T(8,128)} %param.16) | copy-start | bytes 3145732
  7.2 55.5 %copy-start.4 = (f32[4]{0:T(128)S(1)}, f32[4]{0:T(128)}, u32[]{:S(2)}) copy-start(f32[4]{0:T(128)} %param.24) | copy-start | bytes 52
  7.2 53.4 %all-reduce.8.cloned.1.call-start = ((), (), s32[]{:S(2)}) async-start(), calls=%async_computation.6 | async-start | bytes 230400
  18.2 45.8 %copy-start.5 = (f32[128]{0:T(128)S(1)}, f32[128]{0:T(128)}, u32[]{:S(2)}) copy-start(f32[128]{0:T(128)} %param.25) | copy-start | bytes 1540
  21.9 57.6 %copy-start.3 = (bf16[512]{0:T(512)(128)(2,1)S(1)}, bf16[512]{0:T(512)(128)(2,1)}, u32[]{:S(2)}) copy-start(bf16[512]{0:T(512)(128)(2,1)} %param.27) | copy-start | bytes 3076
  21.9 78.2 %copy-start.2 = (bf16[16,128]{1,0:T(8,128)(2,1)S(1)}, bf16[16,128]{1,0:T(8,128)(2,1)}, u32[]{:S(2)}) copy-start(bf16[16,128]{1,0:T(8,128)(2,1)} %param.15) | copy-start | bytes 12292
  23.8 75.5 %reduce-scatter.10.cloned.1.call-start = ((), (), s32[]{:S(2)}) async-start(), calls=%async_computation.4 | async-start | bytes 163840
  79.5 46.5 %reduce-scatter.8.cloned.1.call-start = ((), (), s32[]{:S(2)}) async-start(), calls=%async_computation.3 | async-start | bytes 163840 | tf_op jit(solution)/shard_map/reduce_scatter | solution.py:110
  106.4 54.3 %reduce-scatter.12.cloned.1.call-start = ((), (), s32[]{:S(2)}) async-start(), calls=%async_computation.5 | async-start | bytes 163840
Sparse Core Ops, SparseCore 0:
  23.9 36.6 all-reduce.7
  79.6 19.6 reduce-scatter.9
  106.5 19.4 reduce-scatter.7
  142.8 17.8 reduce-scatter.11
where the time goes:
time: 169 us
  waiting for transfers between devices  78.4 us (46%)
  blocking collectives  49.8 us (29%)
  between operations  14.5 us (9%)
  matrix products  13.2 us (8%)
  other arithmetic  7.94 us (5%)
  local copies, waits for them, and re-layouts  4.54 us (3%)
    unnamed x7, waiting for transfers between devices  70.7 us
    all_gather x1, blocking collectives, local(): head_part = dotted(lax.all_gather(normed, 'kv', axis=0, tiled=True), w_out)  13.3 us
    all_gather x1, blocking collectives, local(): lax.all_gather(hidden_share, 'kv', axis=1, tiled=True)  13.1 us
    dot_general x8, matrix products, dotted(): return jnp.dot(left, right, preferred_element_type=jnp.float32)  12.7 us
    psum x1, blocking collectives, local(): square_two = lax.psum(jnp.sum(middle_rows * middle_rows, axis=1), 'kv')  11.7 us
    reduce_scatter x1, waiting for transfers between devices, local(): up_share = lax.psum_scatter(up_part, 'kv', scatter_dimension=1, tiled=True)  7.72 us
    all_gather x1, blocking collectives, local(): gathered = lax.all_gather(tokens, 'tp', axis=1, tiled=True)  6.51 us
    all_gather x1, blocking collectives, local(): lax.all_gather(middle, 'tp', axis=1, tiled=True).astype(jnp.float32)  5.17 us
  transfers between devices with their start and end apart: 4, of which 4 were waited for; matrix products, arithmetic and copies ran while one was open for 2% of the time, Pallas kernels for 0%

commit v1 on v0

--- a/solution.py
+++ b/solution.py
@@ -1,10 +1,13 @@
+import functools
+
 import jax
 import jax.numpy as jnp
 from jax import lax
+from jax.experimental import pallas as pl
+from jax.experimental.pallas import tpu as pltpu
 from jax.sharding import PartitionSpec as P
 
-D = 2048
-
+MESH = pl.DeviceIdType.MESH
 
 epsilon = 1e-06
 
@@ -34,7 +37,7 @@
     return (normed.astype(jnp.bfloat16), new_state)
 
 
-def local(
+def by_collectives(
     tokens,
     state,
     norm_gain,
@@ -58,6 +61,7 @@
     tp_index = lax.axis_index("tp")
     gathered = lax.all_gather(tokens, "tp", axis=1, tiled=True)
     block = gathered.shape[1]
+    width = block * lax.axis_size("kv")
     inputs = gathered.astype(jnp.float32)
     scaled = (inputs * norm_gain.astype(jnp.float32)).astype(jnp.bfloat16)
     partial_sq = jnp.sum(inputs * inputs, axis=1)
@@ -81,7 +85,7 @@
         lax.psum_scatter(beta_part, "kv", scatter_dimension=0, tiled=True),
         lax.psum_scatter(decay_part, "kv", scatter_dimension=0, tiled=True),
     )
-    first = lax.rsqrt(square_sum / D + epsilon)[:, None]
+    first = lax.rsqrt(square_sum / width + epsilon)[:, None]
     query_pre = (first * query_sum).reshape(seq_here, heads_here, head_size)
     key_pre = (first * key_sum).reshape(seq_here, heads_here, head_size)
     value_pre = (first * value_sum).reshape(seq_here, heads_here, head_size)
@@ -104,7 +108,7 @@
     middle = (tokens.astype(jnp.float32) + attended).astype(jnp.bfloat16)
     middle_rows = lax.all_gather(middle, "tp", axis=1, tiled=True).astype(jnp.float32)
     square_two = lax.psum(jnp.sum(middle_rows * middle_rows, axis=1), "kv")
-    second = lax.rsqrt(square_two / D + epsilon)[:, None]
+    second = lax.rsqrt(square_two / width + epsilon)[:, None]
     scaled_two = (middle_rows * mixer_gain.astype(jnp.float32)).astype(jnp.bfloat16)
     up_part = dotted(scaled_two, w_up)
     up_share = lax.psum_scatter(up_part, "kv", scatter_dimension=1, tiled=True)
@@ -117,9 +121,390 @@
     return (mixed, new_state)
 
 
+def across(left, right):
+    return lax.dot_general(
+        left, right, (((1,), (1,)), ((), ())), preferred_element_type=jnp.float32
+    )
+
+
+def layer_kernel(
+    n_kv,
+    n_tp,
+    tokens,
+    state,
+    norm_gain,
+    w_query,
+    w_key,
+    w_value,
+    w_beta,
+    w_decay,
+    a_log,
+    dt_bias,
+    head_gain,
+    w_out,
+    mixer_gain,
+    w_up,
+    w_down,
+    mixed,
+    new_state,
+    token_all,
+    gain_one,
+    gain_two,
+    gain_head,
+    query_w,
+    key_w,
+    value_w,
+    beta_w,
+    decay_w,
+    out_w,
+    up_w,
+    down_w,
+    states,
+    states_low,
+    log_s,
+    bias_s,
+    qkv_send,
+    qkv_recv,
+    norm_all,
+    part_all,
+    middle_all,
+    up_send,
+    up_recv,
+    hidden_all,
+    down_send,
+    down_recv,
+    mixed_v,
+    load_sem,
+    store_sem,
+    tp_send_sem,
+    tp_recv_sem,
+    kv_send_sem,
+    kv_recv_sem,
+):
+    f32, bf16 = jnp.float32, jnp.bfloat16
+    kv = lax.axis_index("kv")
+    tp = lax.axis_index("tp")
+    rows, feats = tokens.shape
+    block = n_tp * feats
+    seqs, heads, size = state.shape[:3]
+    pairs = seqs * heads
+    all_heads = w_beta.shape[0]
+    share = w_up.shape[1] // n_kv
+    width = block * n_kv
+
+    barrier = pltpu.get_barrier_semaphore()
+    for off in range(1, n_tp):
+        pl.semaphore_signal(
+            barrier, inc=1, device_id={"tp": lax.rem(tp + off, n_tp)}, device_id_type=MESH
+        )
+    for off in range(1, n_kv):
+        pl.semaphore_signal(
+            barrier, inc=1, device_id={"kv": lax.rem(kv + off, n_kv)}, device_id_type=MESH
+        )
+
+    my_rows = pl.ds(pl.multiple_of(kv * block, block), block)
+    loads = {}
+    for number, (name, source, target) in enumerate(
+        (
+            ("tokens", tokens, token_all.at[tp]),
+            ("gain_one", norm_gain, gain_one),
+            ("query", w_query, query_w),
+            ("key", w_key, key_w),
+            ("value", w_value, value_w),
+            ("beta", w_beta.at[:, my_rows], beta_w),
+            ("decay", w_decay.at[:, my_rows], decay_w),
+            ("log", a_log, log_s),
+            ("bias", dt_bias, bias_s),
+            ("gain_head", head_gain, gain_head),
+            ("state", state, states),
+            ("out", w_out, out_w),
+            ("gain_two", mixer_gain, gain_two),
+            ("up", w_up, up_w),
+            ("down", w_down, down_w),
+        )
+    ):
+        loads[name] = pltpu.make_async_copy(source, target, load_sem.at[number])
+        loads[name].start()
+
+    sends = []
+
+    def over_tp(stage, off, source, target):
+        copy = pltpu.make_async_remote_copy(
+            src_ref=source,
+            dst_ref=target,
+            send_sem=tp_send_sem.at[stage, off - 1],
+            recv_sem=tp_recv_sem.at[stage, off - 1],
+            device_id={"tp": lax.rem(tp + off, n_tp)},
+            device_id_type=MESH,
+        )
+        return copy
+
+    def over_kv(stage, off, source, target):
+        copy = pltpu.make_async_remote_copy(
+            src_ref=source,
+            dst_ref=target,
+            send_sem=kv_send_sem.at[stage, off - 1],
+            recv_sem=kv_recv_sem.at[stage, off - 1],
+            device_id={"kv": lax.rem(kv + off, n_kv)},
+            device_id_type=MESH,
+        )
+        return copy
+
+    def gather(over, stage, here, count, slots):
+        for off in range(1, count):
+            copy = over(stage, off, slots.at[here], slots.at[here])
+            copy.start()
+            sends.append(copy)
+
+    def arrived(over, stage, off, here, count, slots):
+        origin = lax.rem(here + count - off, count)
+        over(stage, off, slots.at[origin], slots.at[origin]).wait_recv()
+        return origin
+
+    loads["tokens"].wait()
+    pl.semaphore_wait(barrier, n_tp + n_kv - 2)
+
+    gather(over_tp, 0, tp, n_tp, token_all)
+    for name in ("gain_one", "query", "key", "value", "beta", "decay", "log", "bias", "gain_head"):
+        loads[name].wait()
+    for off in range(1, n_tp):
+        arrived(over_tp, 0, off, tp, n_tp, token_all)
+    inputs = jnp.concatenate([token_all[t].astype(f32) for t in range(n_tp)], axis=1)
+    scaled = (inputs * gain_one[...].astype(f32)).astype(bf16)
+    square = jnp.sum(inputs * inputs, axis=1, keepdims=True)
+    side = jnp.concatenate(
+        [
+            across(scaled, beta_w[...]),
+            across(scaled, decay_w[...]),
+            square,
+            jnp.zeros((rows, 64 - 2 * all_heads - 1), f32),
+        ],
+        axis=1,
+    )
+    side_high = side.astype(bf16).astype(f32)
+    side = jnp.concatenate([side_high, side - side_high], axis=1)
+    parts = [dotted(scaled, w[...]) for w in (query_w, key_w, value_w)]
+    pad = jnp.zeros((16 - seqs, 128), f32)
+    for dest in range(n_kv):
+        at = slice(dest * seqs, (dest + 1) * seqs)
+        pieces = [p[at, h * size : (h + 1) * size] for p in parts for h in range(heads)]
+        qkv_send[dest] = jnp.concatenate(pieces + [side[at], pad], axis=0).astype(bf16)
+    for off in range(1, n_kv):
+        copy = over_kv(0, off, qkv_send.at[lax.rem(kv + off, n_kv)], qkv_recv.at[off - 1])
+        copy.start()
+        sends.append(copy)
+
+    loads["state"].wait()
+    for b in range(seqs):
+        for h in range(heads):
+            states_low[h * seqs + b] = states[b, h].astype(bf16)
+    total = qkv_send[kv].astype(f32)
+    for off in range(1, n_kv):
+        over_kv(0, off, qkv_recv.at[off - 1], qkv_recv.at[off - 1]).wait_recv()
+        total = total + qkv_recv[off - 1].astype(f32)
+
+    lane = lax.rem(lax.broadcasted_iota(jnp.int32, (pairs, 128), 1), 64)
+    head = lax.broadcasted_iota(jnp.int32, (pairs, 128), 0) // seqs
+    side = jnp.concatenate([total[3 * pairs : 3 * pairs + seqs]] * heads, axis=0)
+
+    def column(index):
+        return jnp.sum(jnp.where(lane == index, side, 0.0), axis=1, keepdims=True)
+
+    head_one = lax.broadcasted_iota(jnp.int32, (pairs, 1), 0) // seqs
+    log_rate = jnp.zeros((pairs, 1), f32)
+    bias = jnp.zeros((pairs, 1), f32)
+    for h in range(heads):
+        log_rate = jnp.where(head_one == h, log_s[h], log_rate)
+        bias = jnp.where(head_one == h, bias_s[h], bias)
+    first = lax.rsqrt(column(2 * all_heads) / width + epsilon)
+    logit = first * column(tp * heads + head)
+    beta = 1.0 / (1.0 + jnp.exp(-logit))
+    gate = first * column(all_heads + tp * heads + head) + bias
+    softplus = jnp.maximum(gate, 0.0) + jnp.log1p(jnp.exp(-jnp.abs(gate)))
+    decay = jnp.exp(-jnp.exp(log_rate) * softplus)
+    query_pre = first * total[:pairs]
+    key_pre = first * total[pairs : 2 * pairs]
+    value_pre = first * total[2 * pairs : 3 * pairs]
+    query = query_pre * lax.rsqrt(jnp.sum(query_pre * query_pre, axis=1, keepdims=True) + epsilon)
+    keyed = key_pre * lax.rsqrt(jnp.sum(key_pre * key_pre, axis=1, keepdims=True) + epsilon)
+    both = jnp.concatenate([keyed, query], axis=0).astype(bf16)
+    pair = lax.rem(lax.broadcasted_iota(jnp.int32, (2 * pairs, size), 0), pairs)
+    reads = jnp.zeros((2 * pairs, size), f32)
+    for r in range(pairs):
+        reads = jnp.where(pair == r, dotted(both, states_low[r]), reads)
+    fresh = beta * (value_pre - decay * reads[:pairs])
+    overlap = jnp.sum(query * keyed, axis=1, keepdims=True)
+    reading = decay * reads[pairs:] + overlap * fresh
+    scale = lax.rsqrt(jnp.sum(reading * reading, axis=1, keepdims=True) / size + epsilon)
+    norm_all[kv] = (reading * scale * gain_head[...]).astype(bf16)
+    gather(over_kv, 1, kv, n_kv, norm_all)
+
+    key_columns = keyed.T
+    for r in range(pairs):
+        b, h = r % seqs, r // seqs
+        outer = key_columns[:, r : r + 1] * fresh[r : r + 1, :]
+        states[b, h] = decay[r : r + 1, :] * states[b, h] + outer
+    store_state = pltpu.make_async_copy(states, new_state, store_sem.at[0])
+    store_state.start()
+    for name in ("out", "gain_two", "up", "down"):
+        loads[name].wait()
+
+    for off in range(1, n_kv):
+        arrived(over_kv, 1, off, kv, n_kv, norm_all)
+    normed = [norm_all[k].astype(f32) for k in range(n_kv)]
+    normed = jnp.concatenate(
+        [
+            jnp.concatenate([x[h * seqs : (h + 1) * seqs] for x in normed], axis=0)
+            for h in range(heads)
+        ],
+        axis=1,
+    ).astype(bf16)
+    part_all[tp] = dotted(normed, out_w[...]).astype(bf16)
+    gather(over_tp, 1, tp, n_tp, part_all)
+    for off in range(1, n_tp):
+        arrived(over_tp, 1, off, tp, n_tp, part_all)
+    attended = part_all[0].astype(f32)
+    for t in range(1, n_tp):
+        attended = attended + part_all[t].astype(f32)
+    inputs = jnp.concatenate([token_all[t].astype(f32) for t in range(n_tp)], axis=1)
+    middle = (inputs + attended).astype(bf16).astype(f32)
+    for t in range(n_tp):
+        middle_all[t] = middle[:, t * feats : (t + 1) * feats]
+    square = jnp.sum(middle * middle, axis=1, keepdims=True)
+    square_high = square.astype(bf16).astype(f32)
+    lane = lax.broadcasted_iota(jnp.int32, (rows, 128), 1)
+    square_pair = jnp.where(
+        lane == 0, square_high, jnp.where(lane == 1, square - square_high, 0.0)
+    ).astype(bf16)
+    scaled = (middle * gain_two[...].astype(f32)).astype(bf16)
+
+    def up_block(dest):
+        at = pl.ds(pl.multiple_of(dest * share, share), share)
+        return dotted(scaled, up_w[:, at])
+
+    for off in range(1, n_kv):
+        dest = lax.rem(kv + off, n_kv)
+        up_send[off - 1, :, :share] = up_block(dest).astype(bf16)
+        up_send[off - 1, :, share:] = square_pair
+        copy = over_kv(2, off, up_send.at[off - 1], up_recv.at[off - 1])
+        copy.start()
+        sends.append(copy)
+    up = up_block(kv)
+    pair_sum = square_pair.astype(f32)
+    for off in range(1, n_kv):
+        over_kv(2, off, up_recv.at[off - 1], up_recv.at[off - 1]).wait_recv()
+        up = up + up_recv[off - 1, :, :share].astype(f32)
+        pair_sum = pair_sum + up_recv[off - 1, :, share:].astype(f32)
+    second = lax.rsqrt(jnp.sum(pair_sum, axis=1, keepdims=True) / width + epsilon)
+    hidden_all[kv] = jnp.square(jnp.maximum(second * up, 0.0)).astype(bf16)
+    gather(over_kv, 3, kv, n_kv, hidden_all)
+
+    def down_block(source):
+        at = pl.ds(pl.multiple_of(source * share, share), share)
+        return dotted(hidden_all[source], down_w[at, :])
+
+    down = down_block(kv)
+    for off in range(1, n_kv):
+        down = down + down_block(arrived(over_kv, 3, off, kv, n_kv, hidden_all))
+    for t in range(n_tp):
+        down_send[t] = down[:, t * feats : (t + 1) * feats].astype(bf16)
+    for off in range(1, n_tp):
+        copy = over_tp(2, off, down_send.at[lax.rem(tp + off, n_tp)], down_recv.at[off - 1])
+        copy.start()
+        sends.append(copy)
+    lowered = down_send[tp].astype(f32)
+    for off in range(1, n_tp):
+        over_tp(2, off, down_recv.at[off - 1], down_recv.at[off - 1]).wait_recv()
+        lowered = lowered + down_recv[off - 1].astype(f32)
+    mixed_v[...] = (middle_all[tp] + lowered).astype(bf16)
+    store_mixed = pltpu.make_async_copy(mixed_v, mixed, store_sem.at[1])
+    store_mixed.start()
+    for copy in sends:
+        copy.wait_send()
+    store_state.wait()
+    store_mixed.wait()
+
+
+def local(n_kv, n_tp, *arrays):
+    tokens, state, w_beta, w_up = arrays[0], arrays[1], arrays[6], arrays[13]
+    rows, feats = tokens.shape
+    seqs, heads, size = state.shape[:3]
+    pairs = seqs * heads
+    share = w_up.shape[1] // n_kv
+    aligned = (
+        rows % 16 == 0
+        and feats % 128 == 0
+        and size == 128
+        and pairs % 16 == 0
+        and seqs <= 16
+        and seqs * n_kv == rows
+        and 2 * w_beta.shape[1] < 64
+        and share % 128 == 0
+        and n_kv > 1
+        and n_tp > 1
+    )
+    if not aligned:
+        return by_collectives(*arrays)
+    block = n_tp * feats
+    bf16, f32 = jnp.bfloat16, jnp.float32
+    vmem = pltpu.VMEM
+
+    def held(array):
+        return vmem(array.shape, array.dtype)
+
+    norm_gain, w_query, w_key, w_value = arrays[2:6]
+    head_gain, w_out, mixer_gain, w_up, w_down = arrays[10:]
+    dma = pltpu.SemaphoreType.DMA
+    return pl.pallas_call(
+        functools.partial(layer_kernel, n_kv, n_tp),
+        out_shape=(
+            jax.ShapeDtypeStruct(tokens.shape, tokens.dtype),
+            jax.ShapeDtypeStruct(state.shape, state.dtype),
+        ),
+        in_specs=[pl.BlockSpec(memory_space=pl.ANY)] * len(arrays),
+        out_specs=(pl.BlockSpec(memory_space=pl.ANY),) * 2,
+        scratch_shapes=[
+            vmem((n_tp, rows, feats), bf16),
+            held(norm_gain),
+            held(mixer_gain),
+            held(head_gain),
+            held(w_query),
+            held(w_key),
+            held(w_value),
+            vmem((w_beta.shape[1], block), bf16),
+            vmem((w_beta.shape[1], block), bf16),
+            held(w_out),
+            held(w_up),
+            held(w_down),
+            held(state),
+            vmem((pairs, size, size), bf16),
+            pltpu.SMEM((heads,), f32),
+            pltpu.SMEM((heads,), f32),
+            vmem((n_kv, 3 * pairs + 16, size), bf16),
+            vmem((n_kv - 1, 3 * pairs + 16, size), bf16),
+            vmem((n_kv, pairs, size), bf16),
+            vmem((n_tp, rows, block), bf16),
+            vmem((n_tp, rows, feats), f32),
+            vmem((n_kv - 1, rows, share + 128), bf16),
+            vmem((n_kv - 1, rows, share + 128), bf16),
+            vmem((n_kv, rows, share), bf16),
+            vmem((n_tp, rows, feats), bf16),
+            vmem((n_tp - 1, rows, feats), bf16),
+            vmem((rows, feats), bf16),
+            dma((15,)),
+            dma((2,)),
+            dma((3, n_tp - 1)),
+            dma((3, n_tp - 1)),
+            dma((4, n_kv - 1)),
+            dma((4, n_kv - 1)),
+        ],
+        compiler_params=pltpu.CompilerParams(collective_id=0, has_side_effects=True),
+    )(*arrays[:6], arrays[6].T, arrays[7].T, *arrays[8:])
+
+
 def solution(mesh):
     return jax.shard_map(
-        local,
+        functools.partial(local, mesh.shape["kv"], mesh.shape["tp"]),
         mesh=mesh,
         in_specs=(
             P("grp", ("kv", "tp")),

time: 169 us -> 36.3 us (0.21)
  waiting for transfers between devices: 78.4 us -> 0 us
  blocking collectives: 49.8 us -> 0 us
  Pallas kernels: 0 us -> 31.9 us
  between operations: 14.5 us -> 0.64 us
  matrix products: 13.2 us -> 0 us
  other arithmetic: 7.94 us -> 0 us
    unnamed x7 -> x0, waiting for transfers between devices: 70.7 us -> none
    all_gather x4 -> x0, blocking collectives: 38.1 us -> none  [the longest x1 13.3 us: local(): head_part = dotted(lax.all_gather(normed, 'kv', axis=0, tiled=True), w_out)]
    pallas_call x0 -> x1, Pallas kernels: none -> 31.9 us  [local(): pl.pallas_call(functools.partial(layer_kernel, n_kv, n_tp), out_shape=(ja...]
    dot_general x10 -> x0, matrix products: 13.2 us -> none  [the longest x8 12.7 us: dotted(): return jnp.dot(left, right, preferred_element_type=jnp.float32)]
    psum x1 -> x0, blocking collectives: 11.7 us -> none  [local(): square_two = lax.psum(jnp.sum(middle_rows * middle_rows, axis=1), 'kv')]
    reduce_scatter x1 -> x0, waiting for transfers between devices: 7.72 us -> none  [local(): up_share = lax.psum_scatter(up_part, 'kv', scatter_dimension=1, tiled=True)]
    convert_element_type x6 -> x0, other arithmetic: 2.39 us -> none  [the longest x1 0.83 us: local(): scaled = (inputs * norm_gain.astype(jnp.float32)).astype(jnp.bfloat16)]
    unnamed x19 -> x2, local copies, waits for them, and re-layouts: 4.49 us -> 3.57 us
  transfers between devices with their start and end apart: 4 -> 0, of which waited for: 4 -> 0; matrix products, arithmetic and copies ran while one was open for 2% -> 0% of each run, Pallas kernels for 0% -> 0%
where the time goes in v1:
time: 36.3 us; the launch traced here: 36.1 us
  Pallas kernels  31.9 us (88%)
  local copies, waits for them, and re-layouts  3.57 us (10%)
  between operations  0.64 us (2%)
    pallas_call x1, Pallas kernels, local(): pl.pallas_call(functools.partial(layer_kernel, n_kv, n_tp), out_shape=(ja...  31.9 us
    unnamed x2, local copies, waits for them, and re-layouts  3.57 us

profile of v1, /device:TPU:0, one launch (start us, length us, event | category | flops | bytes accessed | tf_op | source)
XLA Modules:
  0.0 36.1 jit_solution(1099562121746946450)
XLA Ops:
  0.6 31.9 %shard_map.158 = (bf16[16,128]{1,0:T(8,128)(2,1)}, f32[4,4,128,128]{3,2,1,0:T(8,128)}) custom-call(bf16[16,128]{1,0:T(8,128)(2,1)} %tokens.1, f32[4,4,128,128]{3,2,1,0:T(8,128)} %state.1, bf16[512]{0:T(512)(128)(2,1)} %norm_gain.1, bf16[512,512]{1,0:T(8,128)(2,1)} %w_query.1, bf16[512,512]{1,0:T(8,128)(2,1)} %w_key.1, bf16[512,512]{1,0:T(8,128)(2,1)} %w_value.1, ...), custom_call_target="tpu_custom_call" | custom-call | tf_op jit(solution)/shard_map/pallas_call | solution.py:458
  32.5 1.3 %copy.19 = bf16[16,128]{1,0:T(8,128)(2,1)} copy(bf16[16,128]{1,0:T(8,128)(2,1)} %get-tuple-element.4) | data formatting | bytes 8192
  33.8 2.3 %copy.20 = f32[4,4,128,128]{3,2,1,0:T(8,128)} copy(f32[4,4,128,128]{3,2,1,0:T(8,128)} %get-tuple-element.5) | data formatting | bytes 2097152

commit v2 on v1

--- a/solution.py
+++ b/solution.py
@@ -173,9 +173,7 @@
     hidden_all,
     down_send,
     down_recv,
-    mixed_v,
     load_sem,
-    store_sem,
     tp_send_sem,
     tp_recv_sem,
     kv_send_sem,
@@ -343,9 +341,7 @@
     for r in range(pairs):
         b, h = r % seqs, r // seqs
         outer = key_columns[:, r : r + 1] * fresh[r : r + 1, :]
-        states[b, h] = decay[r : r + 1, :] * states[b, h] + outer
-    store_state = pltpu.make_async_copy(states, new_state, store_sem.at[0])
-    store_state.start()
+        new_state[b, h] = decay[r : r + 1, :] * states[b, h] + outer
     for name in ("out", "gain_two", "up", "down"):
         loads[name].wait()
 
@@ -416,13 +412,20 @@
     for off in range(1, n_tp):
         over_tp(2, off, down_recv.at[off - 1], down_recv.at[off - 1]).wait_recv()
         lowered = lowered + down_recv[off - 1].astype(f32)
-    mixed_v[...] = (middle_all[tp] + lowered).astype(bf16)
-    store_mixed = pltpu.make_async_copy(mixed_v, mixed, store_sem.at[1])
-    store_mixed.start()
+    mixed[...] = (middle_all[tp] + lowered).astype(bf16)
     for copy in sends:
         copy.wait_send()
-    store_state.wait()
-    store_mixed.wait()
+
+
+def write_kernel(mixed_v, state_v, mixed, new_state, sem):
+    copies = [
+        pltpu.make_async_copy(mixed_v, mixed, sem.at[0]),
+        pltpu.make_async_copy(state_v, new_state, sem.at[1]),
+    ]
+    for copy in copies:
+        copy.start()
+    for copy in copies:
+        copy.wait()
 
 
 def local(n_kv, n_tp, *arrays):
@@ -455,14 +458,11 @@
     norm_gain, w_query, w_key, w_value = arrays[2:6]
     head_gain, w_out, mixer_gain, w_up, w_down = arrays[10:]
     dma = pltpu.SemaphoreType.DMA
-    return pl.pallas_call(
+    results = pl.pallas_call(
         functools.partial(layer_kernel, n_kv, n_tp),
-        out_shape=(
-            jax.ShapeDtypeStruct(tokens.shape, tokens.dtype),
-            jax.ShapeDtypeStruct(state.shape, state.dtype),
-        ),
-        in_specs=[pl.BlockSpec(memory_space=pl.ANY)] * len(arrays),
-        out_specs=(pl.BlockSpec(memory_space=pl.ANY),) * 2,
+        out_shape=(held(tokens), held(state)),
+        in_specs=[pl.BlockSpec(memory_space=pltpu.HBM)] * len(arrays),
+        out_specs=(pl.BlockSpec(memory_space=vmem),) * 2,
         scratch_shapes=[
             vmem((n_tp, rows, feats), bf16),
             held(norm_gain),
@@ -490,16 +490,24 @@
             vmem((n_kv, rows, share), bf16),
             vmem((n_tp, rows, feats), bf16),
             vmem((n_tp - 1, rows, feats), bf16),
-            vmem((rows, feats), bf16),
             dma((15,)),
-            dma((2,)),
             dma((3, n_tp - 1)),
             dma((3, n_tp - 1)),
             dma((4, n_kv - 1)),
             dma((4, n_kv - 1)),
         ],
-        compiler_params=pltpu.CompilerParams(collective_id=0, has_side_effects=True),
+        compiler_params=pltpu.CompilerParams(
+            collective_id=0, has_side_effects=True, vmem_limit_bytes=64 * 2**20 - 65536 - state.size * 4 - 2 * tokens.size
+        ),
     )(*arrays[:6], arrays[6].T, arrays[7].T, *arrays[8:])
+    return pl.pallas_call(
+        write_kernel,
+        out_shape=tuple(jax.ShapeDtypeStruct(r.shape, r.dtype) for r in (tokens, state)),
+        in_specs=[pl.BlockSpec(memory_space=pl.ANY)] * 2,
+        out_specs=(pl.BlockSpec(memory_space=pltpu.HBM),) * 2,
+        scratch_shapes=[dma((2,))],
+        compiler_params=pltpu.CompilerParams(vmem_limit_bytes=2**20),
+    )(*results)
 
 
 def solution(mesh):

time: 36.3 us -> 33.1 us (0.912)
  local copies, waits for them, and re-layouts: 3.57 us -> 0 us
  Pallas kernels: 31.9 us -> 32.3 us
    unnamed x2 -> x0, local copies, waits for them, and re-layouts: 3.57 us -> none
    pallas_call x1 -> x2, Pallas kernels: 31.9 us -> 32.3 us  [the longest x1 31.3 us: local(): pl.pallas_call(functools.partial(layer_kernel, n_kv, n_tp), out_shape=(he...]
where the time goes in v2:
time: 33.1 us; the launch traced here: 32.9 us
  Pallas kernels  32.3 us (98%)
  between operations  0.64 us (2%)
    pallas_call x1, Pallas kernels, local(): pl.pallas_call(functools.partial(layer_kernel, n_kv, n_tp), out_shape=(he...  31.3 us
    pallas_call x1, Pallas kernels, local(): pl.pallas_call(write_kernel, out_shape=tuple((jax.ShapeDtypeStruct(r.shap...  0.99 us

profile of v2, /device:TPU:0, one launch (start us, length us, event | category | flops | bytes accessed | tf_op | source)
XLA Modules:
  0.0 32.9 jit_solution(1380846419557849893)
XLA Ops:
  0.6 31.3 %shard_map.158 = (bf16[16,128]{1,0:T(8,128)(2,1)S(1)}, f32[4,4,128,128]{3,2,1,0:T(8,128)S(1)}) custom-call(bf16[16,128]{1,0:T(8,128)(2,1)} %tokens.1, f32[4,4,128,128]{3,2,1,0:T(8,128)} %state.1, bf16[512]{0:T(512)(128)(2,1)} %norm_gain.1, bf16[512,512]{1,0:T(8,128)(2,1)} %w_query.1, bf16[512,512]{1,0:T(8,128)(2,1)} %w_key.1, bf16[512,512]{1,0:T(8,128)(2,1)} %w_value.1, ...), custom_call_target="tpu_custom_call" | custom-call | tf_op jit(solution)/shard_map/pallas_call | solution.py:461
  32.0 1.0 %shard_map.159 = (bf16[16,128]{1,0:T(8,128)(2,1)}, f32[4,4,128,128]{3,2,1,0:T(8,128)}) custom-call(bf16[16,128]{1,0:T(8,128)(2,1)S(1)} %get-tuple-element.4.mixed_v, f32[4,4,128,128]{3,2,1,0:T(8,128)S(1)} %get-tuple-element.5.state_v), custom_call_target="tpu_custom_call" | custom-call | tf_op jit(solution)/shard_map/pallas_call | solution.py:503

commit v3 on v2

--- a/solution.py
+++ b/solution.py
@@ -178,6 +178,7 @@
     tp_recv_sem,
     kv_send_sem,
     kv_recv_sem,
+    news_sem,
 ):
     f32, bf16 = jnp.float32, jnp.bfloat16
     kv = lax.axis_index("kv")
@@ -195,10 +196,36 @@
         pl.semaphore_signal(
             barrier, inc=1, device_id={"tp": lax.rem(tp + off, n_tp)}, device_id_type=MESH
         )
-    for off in range(1, n_kv):
-        pl.semaphore_signal(
-            barrier, inc=1, device_id={"kv": lax.rem(kv + off, n_kv)}, device_id_type=MESH
-        )
+    last = n_kv - 1
+    for step in (-1, 1):
+
+        @pl.when((kv + step >= 0) & (kv + step <= last))
+        def _(step=step):
+            pl.semaphore_signal(barrier, inc=1, device_id={"kv": kv + step}, device_id_type=MESH)
+
+    turn = jnp.where(2 * kv >= n_kv, 1, -1)
+    kv_offs = [lax.rem(n_kv + turn * j, n_kv) for j in range(1, n_kv)]
+
+    def tell(far):
+        for side, step in enumerate((-1, 1)):
+
+            @pl.when((kv + step >= 0) & (kv + step <= last))
+            def _(side=side, step=step):
+                @pl.when((kv - far * step >= 0) & (kv - far * step <= last))
+                def _():
+                    pl.semaphore_signal(
+                        news_sem.at[far - 1, side],
+                        inc=1,
+                        device_id={"kv": kv + step},
+                        device_id_type=MESH,
+                    )
+
+    def hear(far):
+        for side, step in enumerate((-1, 1)):
+
+            @pl.when((kv - (far + 1) * step >= 0) & (kv - (far + 1) * step <= last))
+            def _(side=side):
+                pl.semaphore_wait(news_sem.at[far - 1, side], 1)
 
     my_rows = pl.ds(pl.multiple_of(kv * block, block), block)
     loads = {}
@@ -248,8 +275,8 @@
         )
         return copy
 
-    def gather(over, stage, here, count, slots):
-        for off in range(1, count):
+    def gather(over, stage, here, offs, slots):
+        for off in offs:
             copy = over(stage, off, slots.at[here], slots.at[here])
             copy.start()
             sends.append(copy)
@@ -260,9 +287,14 @@
         return origin
 
     loads["tokens"].wait()
-    pl.semaphore_wait(barrier, n_tp + n_kv - 2)
-
-    gather(over_tp, 0, tp, n_tp, token_all)
+    neighbours = jnp.where(kv > 0, 1, 0) + jnp.where(kv < last, 1, 0)
+    pl.semaphore_wait(barrier, n_tp - 1 + neighbours)
+
+    gather(over_tp, 0, tp, range(1, n_tp), token_all)
+    for far in range(1, n_kv - 1):
+        tell(far)
+        if far < n_kv - 2:
+            hear(far)
     for name in ("gain_one", "query", "key", "value", "beta", "decay", "log", "bias", "gain_head"):
         loads[name].wait()
     for off in range(1, n_tp):
@@ -287,7 +319,9 @@
         at = slice(dest * seqs, (dest + 1) * seqs)
         pieces = [p[at, h * size : (h + 1) * size] for p in parts for h in range(heads)]
         qkv_send[dest] = jnp.concatenate(pieces + [side[at], pad], axis=0).astype(bf16)
-    for off in range(1, n_kv):
+    if n_kv > 2:
+        hear(n_kv - 2)
+    for off in kv_offs:
         copy = over_kv(0, off, qkv_send.at[lax.rem(kv + off, n_kv)], qkv_recv.at[off - 1])
         copy.start()
         sends.append(copy)
@@ -297,7 +331,7 @@
         for h in range(heads):
             states_low[h * seqs + b] = states[b, h].astype(bf16)
     total = qkv_send[kv].astype(f32)
-    for off in range(1, n_kv):
+    for off in kv_offs:
         over_kv(0, off, qkv_recv.at[off - 1], qkv_recv.at[off - 1]).wait_recv()
         total = total + qkv_recv[off - 1].astype(f32)
 
@@ -335,7 +369,7 @@
     reading = decay * reads[pairs:] + overlap * fresh
     scale = lax.rsqrt(jnp.sum(reading * reading, axis=1, keepdims=True) / size + epsilon)
     norm_all[kv] = (reading * scale * gain_head[...]).astype(bf16)
-    gather(over_kv, 1, kv, n_kv, norm_all)
+    gather(over_kv, 1, kv, kv_offs, norm_all)
 
     key_columns = keyed.T
     for r in range(pairs):
@@ -356,7 +390,7 @@
         axis=1,
     ).astype(bf16)
     part_all[tp] = dotted(normed, out_w[...]).astype(bf16)
-    gather(over_tp, 1, tp, n_tp, part_all)
+    gather(over_tp, 1, tp, range(1, n_tp), part_all)
     for off in range(1, n_tp):
         arrived(over_tp, 1, off, tp, n_tp, part_all)
     attended = part_all[0].astype(f32)
@@ -378,7 +412,7 @@
         at = pl.ds(pl.multiple_of(dest * share, share), share)
         return dotted(scaled, up_w[:, at])
 
-    for off in range(1, n_kv):
+    for off in kv_offs:
         dest = lax.rem(kv + off, n_kv)
         up_send[off - 1, :, :share] = up_block(dest).astype(bf16)
         up_send[off - 1, :, share:] = square_pair
@@ -387,20 +421,20 @@
         sends.append(copy)
     up = up_block(kv)
     pair_sum = square_pair.astype(f32)
-    for off in range(1, n_kv):
+    for off in kv_offs:
         over_kv(2, off, up_recv.at[off - 1], up_recv.at[off - 1]).wait_recv()
         up = up + up_recv[off - 1, :, :share].astype(f32)
         pair_sum = pair_sum + up_recv[off - 1, :, share:].astype(f32)
     second = lax.rsqrt(jnp.sum(pair_sum, axis=1, keepdims=True) / width + epsilon)
     hidden_all[kv] = jnp.square(jnp.maximum(second * up, 0.0)).astype(bf16)
-    gather(over_kv, 3, kv, n_kv, hidden_all)
+    gather(over_kv, 3, kv, kv_offs, hidden_all)
 
     def down_block(source):
         at = pl.ds(pl.multiple_of(source * share, share), share)
         return dotted(hidden_all[source], down_w[at, :])
 
     down = down_block(kv)
-    for off in range(1, n_kv):
+    for off in kv_offs:
         down = down + down_block(arrived(over_kv, 3, off, kv, n_kv, hidden_all))
     for t in range(n_tp):
         down_send[t] = down[:, t * feats : (t + 1) * feats].astype(bf16)
@@ -495,6 +529,7 @@
             dma((3, n_tp - 1)),
             dma((4, n_kv - 1)),
             dma((4, n_kv - 1)),
+            pltpu.SemaphoreType.REGULAR((max(n_kv - 2, 1), 2)),
         ],
         compiler_params=pltpu.CompilerParams(
             collective_id=0, has_side_effects=True, vmem_limit_bytes=64 * 2**20 - 65536 - state.size * 4 - 2 * tokens.size

time: 33.1 us -> 30.9 us (0.934)
  Pallas kernels: 32.3 us -> 30.1 us
    pallas_call x1, Pallas kernels: 31.3 us -> 29.1 us  [local(): pl.pallas_call(functools.partial(layer_kernel, n_kv, n_tp), out_shape=(he...]
where the time goes in v3:
time: 30.9 us; the launch traced here: 30.7 us
  Pallas kernels  30.1 us (97%)
  between operations  0.64 us (2%)
    pallas_call x1, Pallas kernels, local(): pl.pallas_call(functools.partial(layer_kernel, n_kv, n_tp), out_shape=(he...  29.1 us
    pallas_call x1, Pallas kernels, local(): pl.pallas_call(write_kernel, out_shape=tuple((jax.ShapeDtypeStruct(r.shap...  0.99 us

profile of v3, /device:TPU:0, one launch (start us, length us, event | category | flops | bytes accessed | tf_op | source)
XLA Modules:
  0.0 30.7 jit_solution(17606017321279063771)
XLA Ops:
  0.6 29.1 %shard_map.158 = (bf16[16,128]{1,0:T(8,128)(2,1)S(1)}, f32[4,4,128,128]{3,2,1,0:T(8,128)S(1)}) custom-call(bf16[16,128]{1,0:T(8,128)(2,1)} %tokens.1, f32[4,4,128,128]{3,2,1,0:T(8,128)} %state.1, bf16[512]{0:T(512)(128)(2,1)} %norm_gain.1, bf16[512,512]{1,0:T(8,128)(2,1)} %w_query.1, bf16[512,512]{1,0:T(8,128)(2,1)} %w_key.1, bf16[512,512]{1,0:T(8,128)(2,1)} %w_value.1, ...), custom_call_target="tpu_custom_call" | custom-call | tf_op jit(solution)/shard_map/pallas_call | solution.py:495
  29.7 1.0 %shard_map.159 = (bf16[16,128]{1,0:T(8,128)(2,1)}, f32[4,4,128,128]{3,2,1,0:T(8,128)}) custom-call(bf16[16,128]{1,0:T(8,128)(2,1)S(1)} %get-tuple-element.4.mixed_v, f32[4,4,128,128]{3,2,1,0:T(8,128)S(1)} %get-tuple-element.5.state_v), custom_call_target="tpu_custom_call" | custom-call | tf_op jit(solution)/shard_map/pallas_call | solution.py:538
